TPU v7x, 256 devices: a whole 4x4x8 slice. The times are simulated.
256 devices in a mesh: sp: 32 (over z, y), tp: 8 (over x, core).
Axes of the slice: x: 4, y: 4, z: 8, core: 2. Of those that a mesh axis runs over, the one named last changes fastest.
Arguments:
- hidden: bfloat16 [24576, 2048], P(('sp', 'tp')), may hold values from -6 to 6
- norm_gain: float32 [2, 2048], replicated, may hold values from 0.1 to 1.9
- w_value: bfloat16 [2, 2048, 2048], P(None, 'sp', 'tp'), may hold values from -0.125 to 0.125
- w_gate: bfloat16 [2, 2048, 2048], P(None, 'sp', 'tp'), may hold values from -0.125 to 0.125
- conv_weight: float32 [2, 31, 2048], P(None, None, 'tp'), may hold values from -3 to 3
- conv_bias: float32 [2, 2048], P(None, 'tp'), may hold values from -3 to 3
- chan_gain: float32 [2, 2048], P(None, 'tp'), may hold values from 0.1 to 1.9
- chan_shift: float32 [2, 2048], P(None, 'tp'), may hold values from -3 to 3
- w_out: bfloat16 [2, 2048, 2048], P(None, 'tp', 'sp'), may hold values from -0.125 to 0.125
Outputs:
- result: bfloat16 [24576, 2048], P(('sp', 'tp'))
All inputs are finite; a program needn't handle non-finite values.
Results may differ from a plain program's by a relative error of at most 0.015.
Values may be sent and summed in bfloat16 or wider, within the bound.
No kernel may reach another device: no remote copies, remote signals or barrier semaphores. Data moves between devices by JAX's collectives and lax.ppermute only.
A program may use at most 64 MiB of HBM per device.

v0:
```python
import jax
import jax.numpy as jnp
from jax import lax
from jax.sharding import Mesh
from jax.sharding import PartitionSpec as P

SP = ("sp_0", "sp_1")
SP_TP = ("sp_0", "sp_1", "tp")
EPS = 1e-06


def sent_together(arrays, axis, dim, along):
    widths = [a.shape[along] for a in arrays]
    both = jnp.concatenate(arrays, axis=along)
    whole = lax.all_gather(both, axis, axis=dim, tiled=True)
    return tuple(jnp.split(whole, [sum(widths[:k]) for k in range(1, len(widths))], axis=along))


def shifted(shard, axis, by):
    size = lax.axis_size(axis)
    pairs = [(i, i + by) for i in range(size) if 0 <= i + by < size]
    return lax.ppermute(shard, axis, pairs)


def sent_to_all(shard, axis):
    size = lax.axis_size(axis)
    return lax.all_to_all(
        jnp.broadcast_to(shard[None], (size, *shard.shape)), axis, 0, 0, tiled=True
    )


def of_everyone(shard, axis):
    everything = sent_to_all(shard, axis)
    return jnp.sum(everything, axis=0)


def together(arrays, axis):
    ravelled, at, finished = (jnp.concatenate([a.reshape(-1) for a in arrays]), 0, [])
    running = of_everyone(ravelled, axis)
    for a in arrays:
        finished.append(running[at : at + a.size].reshape(a.shape))
        at += a.size
    return tuple(finished)


def whole_of(shard, axes, dim):
    if not axes:
        return shard
    nearer = lax.all_gather(shard, axes[-1], axis=dim, tiled=True)
    return whole_of(nearer, axes[:-1], dim)


def cut_along(shard, dim, size):
    dims = shard.shape
    tiles = shard.reshape(*dims[:dim], size, dims[dim] // size, *dims[dim + 1 :])
    return jnp.moveaxis(tiles, dim, 0)


def sum_at_owner(shard, axis, dim):
    tiles = cut_along(shard, dim, lax.axis_size(axis))
    arrived = lax.all_to_all(tiles, axis, split_axis=0, concat_axis=0, tiled=True)
    return arrived.astype(jnp.float32).sum(axis=0)


def body(hidden, norm_gain, w_value, w_gate, conv_weight, conv_bias, chan_gain, chan_shift, w_out):
    group = lax.axis_size("tp")
    own_rows = hidden.shape[0]
    chans = w_value.shape[2]
    taps = conv_weight.shape[1]
    state = hidden
    for layer in range(norm_gain.shape[0]):
        xf = state.astype(jnp.float32)
        scale = lax.rsqrt(jnp.mean(xf * xf, axis=1, keepdims=True) + EPS)
        normed = (xf * scale * norm_gain[layer][None, :]).astype(jnp.bfloat16)
        tokens = lax.all_gather(normed, "tp", axis=0, tiled=True)
        empty = jnp.zeros((tokens.shape[0], chans), jnp.float32)

        def add_both(totals, pieces, start, tokens=tokens):
            return (
                jnp.dot(tokens, pieces[0], preferred_element_type=jnp.float32),
                jnp.dot(tokens, pieces[1], preferred_element_type=jnp.float32),
            )

        lin, gate = add_both(
            (empty, empty), sent_together((w_value[layer], w_gate[layer]), SP, 0, 1), jnp.int32(0)
        )
        glu = (lin * jax.nn.sigmoid(gate)).astype(jnp.bfloat16)
        before = shifted(glu[tokens.shape[0] - (taps - 1) :], SP, 1)
        window = jnp.concatenate([before, glu], axis=0).astype(jnp.float32)
        length = tokens.shape[0]
        mixed = jnp.zeros((length, chans), jnp.float32) + conv_bias[layer][None, :]
        for tap in range(taps):
            mixed = mixed + conv_weight[layer, tap][None, :] * window[tap : tap + length]
        totals = together((jnp.sum(mixed, axis=1), jnp.sum(mixed * mixed, axis=1)), "tp")
        mean = (totals[0] / (chans * group))[:, None]
        msq = (totals[1] / (chans * group))[:, None]
        var = msq - mean * mean
        act = jax.nn.silu(
            (mixed - mean) * lax.rsqrt(var + EPS) * chan_gain[layer][None, :]
            + chan_shift[layer][None, :]
        ).astype(jnp.bfloat16)

        def project(piece, start, act=act):
            return jnp.dot(act, piece, preferred_element_type=jnp.float32)

        partial_out = project(whole_of(w_out[layer], SP, 1), jnp.int32(0))

        def take_rows(start, count, partial_out=partial_out):
            return partial_out

        update = sum_at_owner(
            take_rows(jnp.int32(0), own_rows * lax.axis_size("tp")).astype(jnp.bfloat16), "tp", 0
        )
        state = (xf + update).astype(jnp.bfloat16)
    return state


def solution(mesh):
    torus = Mesh(mesh.devices.reshape(8, 4, mesh.shape["tp"]), ("sp_0", "sp_1", "tp"))
    in_specs = (
        P(SP_TP, None),
        P(),
        P(None, SP, "tp"),
        P(None, SP, "tp"),
        P(None, None, "tp"),
        P(None, "tp"),
        P(None, "tp"),
        P(None, "tp"),
        P(None, "tp", SP),
    )
    out_specs = P(SP_TP, None)
    return jax.shard_map(body, mesh=torus, in_specs=in_specs, out_specs=out_specs, check_vma=False)
```

profile of v0, /device:TPU:1, one launch (start us, length us, event | category | flops | bytes accessed | tf_op | source)
XLA Modules:
  0.0 361.9 jit_solution(7405386278213270947)
XLA Ops:
  8.1 1.2 fusion.14
  9.2 0.8 fusion.112
  10.1 1.9 fusion.16
  12.8 11.2 %all-gather = bf16[1,256,256]{1,2,0:T(8,128)(2,1)} all-gather(bf16[1,256,64]{1,2,0:T(8,128)(2,1)S(1)} %get-tuple-element.17), channel_id=2, replica_groups=mesh['sp_0'=8,'sp_1'=4,'tp'=8] {'sp_1'}, dimensions={2}, use_global_device_ids=true | all-gather | bytes 163840 | tf_op jit(solution)/shard_map/all_gather | solution.py:49
  24.7 0.9 fusion.110
  25.6 0.9 fusion.109
  28.0 59.0 %all-gather.13.cloned.1.call-done = bf16[2048,512]{1,0:T(8,128)(2,1)} async-done(((bf16[64,512]{1,0:T(8,128)(2,1)}), bf16[2048,512]{1,0:T(8,128)(2,1)}) %all-gather.13.cloned.1.call-update) | async-done | bytes 2097168 | tf_op jit(solution)/shard_map/all_gather | solution.py:15
  87.1 34.3 %all-gather.11.cloned.1.call-done = bf16[768,2048]{1,0:T(8,128)(2,1)} async-done(((bf16[96,2048]{1,0:T(8,128)(2,1)}), bf16[768,2048]{1,0:T(8,128)(2,1)}) %all-gather.11.cloned.1.call-update) | async-done | bytes 3145744 | tf_op jit(solution)/shard_map/all_gather | solution.py:75
  121.4 3.3 fusion.3
  124.7 1.0 fusion.6
  125.8 3.1 collective-permute-start
  128.9 0.8 collective-permute-done
  129.8 3.5 fusion.103
  134.0 4.4 %all-to-all-start = ((f32[8,1,1536]{2,1,0:T(1,128)}), f32[8,1,1536]{2,1,0:T(1,128)S(1)}, u32[]{:S(2)}, u32[]{:S(2)}) async-start(f32[8,1,1536]{2,1,0:T(1,128)} %broadcast_in_dim.4), calls=%async_computation | async-start | bytes 98304 | tf_op jit(solution)/shard_map/all_to_all | solution.py:27
  138.4 4.8 %all-to-all-done = f32[8,1,1536]{2,1,0:T(1,128)S(1)} async-done(((f32[8,1,1536]{2,1,0:T(1,128)}), f32[8,1,1536]{2,1,0:T(1,128)S(1)}, u32[]{:S(2)}, u32[]{:S(2)}) %all-to-all-start) | async-done | bytes 49184 | tf_op jit(solution)/shard_map/all_to_all | solution.py:27
  143.3 13.7 %all-gather.19.cloned.1.call-done = bf16[1,256,2048]{1,2,0:T(8,128)(2,1)} async-done(((bf16[1,256,256]{1,2,0:T(8,128)(2,1)}), bf16[1,256,2048]{1,2,0:T(8,128)(2,1)}) %all-gather.19.cloned.1.call-update) | async-done | bytes 1048592 | tf_op jit(solution)/shard_map/all_gather | solution.py:49
  156.9 2.3 convolution_convert_fusion.1
  159.3 46.4 %all_to_all.22 = bf16[8,96,2048]{2,1,0:T(8,128)(2,1)S(1)} all-to-all(bf16[8,96,2048]{2,1,0:T(8,128)(2,1)S(1)} %bitcast.90), channel_id=1, replica_groups=mesh['sp_0'=8,'sp_1'=4,'tp'=8] {'tp'}, dimensions={0} | all-to-all | bytes 6291456 | tf_op jit(solution)/shard_map/all_to_all | solution.py:61
  206.9 0.9 fusion.20
  207.9 11.0 %all-gather.2 = bf16[1,256,256]{1,2,0:T(8,128)(2,1)} all-gather(bf16[1,256,64]{1,2,0:T(8,128)(2,1)S(1)} %get-tuple-element.18), channel_id=4, replica_groups=mesh['sp_0'=8,'sp_1'=4,'tp'=8] {'sp_1'}, dimensions={2}, use_global_device_ids=true | all-gather | bytes 163840 | tf_op jit(solution)/shard_map/all_gather | solution.py:49
  219.0 16.4 %all-gather.17.cloned.1.call-done = bf16[2048,512]{1,0:T(8,128)(2,1)} async-done(((bf16[64,512]{1,0:T(8,128)(2,1)}), bf16[2048,512]{1,0:T(8,128)(2,1)}) %all-gather.17.cloned.1.call-update) | async-done | bytes 2097168 | tf_op jit(solution)/shard_map/all_gather | solution.py:15
  235.4 34.2 %all-gather.15.cloned.1.call-done = bf16[768,2048]{1,0:T(8,128)(2,1)} async-done(((bf16[96,2048]{1,0:T(8,128)(2,1)}), bf16[768,2048]{1,0:T(8,128)(2,1)}) %all-gather.15.cloned.1.call-update) | async-done | bytes 3145744 | tf_op jit(solution)/shard_map/all_gather | solution.py:75
  269.6 3.3 fusion.5
  272.9 1.0 fusion.7
  273.9 3.1 collective-permute-start.1
  277.0 0.9 fusion.108
  278.0 3.5 fusion.102
  281.6 8.6 %all_to_all.23 = f32[8,1,1536]{2,1,0:T(1,128)S(1)} all-to-all(f32[8,1,1536]{2,1,0:T(1,128)S(1)} %broadcast_in_dim.5), channel_id=1, replica_groups=mesh['sp_0'=8,'sp_1'=4,'tp'=8] {'tp'}, dimensions={0} | all-to-all | bytes 98304 | tf_op jit(solution)/shard_map/all_to_all | solution.py:27
  290.3 13.9 %all-gather.21.cloned.1.call-done = bf16[1,256,2048]{1,2,0:T(8,128)(2,1)} async-done(((bf16[1,256,256]{1,2,0:T(8,128)(2,1)}), bf16[1,256,2048]{1,2,0:T(8,128)(2,1)}) %all-gather.21.cloned.1.call-update) | async-done | bytes 1048592 | tf_op jit(solution)/shard_map/all_gather | solution.py:49
  304.2 2.3 convolution_convert_fusion
  306.5 47.1 %all_to_all.24 = bf16[8,96,2048]{2,1,0:T(8,128)(2,1)S(1)} all-to-all(bf16[8,96,2048]{2,1,0:T(8,128)(2,1)S(1)} %bitcast.91), channel_id=1, replica_groups=mesh['sp_0'=8,'sp_1'=4,'tp'=8] {'tp'}, dimensions={0} | all-to-all | bytes 6291456 | tf_op jit(solution)/shard_map/all_to_all | solution.py:61
  354.2 0.8 fusion.21
  (52 shorter events, 7.4 us)
Async XLA Ops:
  6.5 80.5 %all-gather.13.cloned.1.call-start = ((), (), s32[]{:S(2)}) async-start(), calls=%async_computation.5 | async-start | bytes 2162688 | tf_op jit(solution)/shard_map/all_gather | solution.py:15
  8.0 113.4 %all-gather.11.cloned.1.call-start = ((), (), s32[]{:S(2)}) async-start(), calls=%async_computation.4 | async-start | bytes 3538944 | tf_op jit(solution)/shard_map/all_gather | solution.py:75
  12.0 144.9 %all-gather.19.cloned.1.call-start = ((), (), s32[]{:S(2)}) async-start(), calls=%async_computation.8 | async-start | bytes 1179648 | tf_op jit(solution)/shard_map/all_gather | solution.py:49
  24.0 211.3 %all-gather.17.cloned.1.call-start = ((), (), s32[]{:S(2)}) async-start(), calls=%async_computation.7 | async-start | bytes 2162688 | tf_op jit(solution)/shard_map/all_gather | solution.py:15
  87.1 37.6 %copy-start.6 = (bf16[2048,512]{1,0:T(8,128)(2,1)S(1)}, bf16[2048,512]{1,0:T(8,128)(2,1)}, u32[]{:S(2)}) copy-start(bf16[2048,512]{1,0:T(8,128)(2,1)} %all-gather.13.cloned.1.call-done) | copy-start | bytes 6291460
  121.4 3.3 copy-start.3
  124.7 4.2 %copy-start.1 = (f32[2,256]{1,0:T(2,128)S(1)}, f32[2,256]{1,0:T(2,128)}, u32[]{:S(2)}) copy-start(f32[2,256]{1,0:T(2,128)} %param.15) | copy-start | bytes 6148
  125.8 4.0 %collective-permute-start = (bf16[30,256]{1,0:T(8,128)(2,1)S(1)}, bf16[30,256]{1,0:T(8,128)(2,1)S(1)}, u32[]{:S(2)}, u32[]{:S(2)}) collective-permute-start(bf16[30,256]{1,0:T(8,128)(2,1)S(1)} %slice.576), channel_id=1, source_target_pairs={{0,8},{8,16},{16,24},{24,32},{32,40},{40,48},{48,56},{56,64},{64,7... | collective-permute-start | bytes 46088 | tf_op jit(solution)/shard_map/ppermute | solution.py:22
  129.8 8.6 %copy-start.2 = (f32[2,256]{1,0:T(2,128)S(1)}, f32[2,256]{1,0:T(2,128)}, u32[]{:S(2)}) copy-start(f32[2,256]{1,0:T(2,128)} %param.16) | copy-start | bytes 6148
  134.0 9.2 %all-to-all-start = ((f32[8,1,1536]{2,1,0:T(1,128)}), f32[8,1,1536]{2,1,0:T(1,128)S(1)}, u32[]{:S(2)}, u32[]{:S(2)}) async-start(f32[8,1,1536]{2,1,0:T(1,128)} %broadcast_in_dim.4), calls=%async_computation | async-start | bytes 98304 | tf_op jit(solution)/shard_map/all_to_all | solution.py:27
  138.4 131.2 %all-gather.15.cloned.1.call-start = ((), (), s32[]{:S(2)}) async-start(), calls=%async_computation.6 | async-start | bytes 3538944 | tf_op jit(solution)/shard_map/all_gather | solution.py:75
  205.7 1.0 copy-start
  207.8 96.4 %all-gather.21.cloned.1.call-start = ((), (), s32[]{:S(2)}) async-start(), calls=%async_computation.9 | async-start | bytes 1179648 | tf_op jit(solution)/shard_map/all_gather | solution.py:49
  235.4 37.5 %copy-start.5 = (bf16[2048,512]{1,0:T(8,128)(2,1)S(1)}, bf16[2048,512]{1,0:T(8,128)(2,1)}, u32[]{:S(2)}) copy-start(bf16[2048,512]{1,0:T(8,128)(2,1)} %all-gather.17.cloned.1.call-done) | copy-start | bytes 6291460
  269.6 3.3 copy-start.4
  273.9 4.0 %collective-permute-start.1 = (bf16[30,256]{1,0:T(8,128)(2,1)S(1)}, bf16[30,256]{1,0:T(8,128)(2,1)S(1)}, u32[]{:S(2)}, u32[]{:S(2)}) collective-permute-start(bf16[30,256]{1,0:T(8,128)(2,1)S(1)} %slice.610), channel_id=1, source_target_pairs={{0,8},{8,16},{16,24},{24,32},{32,40},{40,48},{48,56},{56,64},{64,7... | collective-permute-start | bytes 46088 | tf_op jit(solution)/shard_map/ppermute | solution.py:22
Sparse Core Ops, SparseCore 0:
  9.9 77.1 all-gather.12
  88.9 32.4 all-gather.10
  123.2 33.7 all-gather.18
  159.4 75.9 all-gather.16
  237.0 32.4 all-gather.14
  271.2 32.9 all-gather.20
where the time goes:
time: 363 us; the launch traced here: 362 us
  waiting for transfers between devices  177 us (49%)
  blocking collectives  124 us (34%)
  other arithmetic  14.7 us (4%)
  between operations  13.7 us (4%)
  matrix products  13.3 us (4%)
  starting transfers between devices  10.8 us (3%)
  local copies, waits for them, and re-layouts  7.75 us (2%)
    all_to_all x2, blocking collectives, sum_at_owner(): lax.all_to_all(tiles, axis, split_axis=0, concat_axis=0, tiled=True)  93.5 us
    all_gather x2, waiting for transfers between devices, sent_together(): whole = lax.all_gather(both, axis, axis=dim, tiled=True)  75.5 us
    all_gather x2, waiting for transfers between devices, body(): tokens = lax.all_gather(normed, 'tp', axis=0, tiled=True)  68.5 us
    all_gather x2, waiting for transfers between devices, whole_of(): nearer = lax.all_gather(shard, axes[-1], axis=dim, tiled=True)  27.6 us
    all_gather x2, blocking collectives, whole_of(): nearer = lax.all_gather(shard, axes[-1], axis=dim, tiled=True)  22.2 us
    all_to_all x1, blocking collectives, sent_to_all(): lax.all_to_all(jnp.broadcast_to(shard[None], (size, *shard.shape)), axis,...  8.63 us
  transfers between devices with their start and end apart: 9, of which 8 were waited for; matrix products, arithmetic and copies ran while one was open for 8% of the time, Pallas kernels for 0%

commit v1 on v0

--- a/solution.py
+++ b/solution.py
@@ -7,6 +7,12 @@
 SP = ("sp_0", "sp_1")
 SP_TP = ("sp_0", "sp_1", "tp")
 EPS = 1e-06
+
+
+def joined_along(pieces, dim):
+    dims = list(pieces.shape[1:])
+    dims[dim] *= pieces.shape[0]
+    return jnp.moveaxis(pieces, 0, dim).reshape(dims)
 
 
 def sent_together(arrays, axis, dim, along):
@@ -72,7 +78,19 @@
         xf = state.astype(jnp.float32)
         scale = lax.rsqrt(jnp.mean(xf * xf, axis=1, keepdims=True) + EPS)
         normed = (xf * scale * norm_gain[layer][None, :]).astype(jnp.bfloat16)
-        tokens = lax.all_gather(normed, "tp", axis=0, tiled=True)
+        devices = lax.axis_size("tp")
+        pairs_2 = [(i_2, (i_2 + 1) % devices) for i_2 in range(devices)]
+        back = [(b, a_2) for a_2, b in pairs_2]
+        lower, upper = ([], [])
+        for step in range(devices - 1):
+            if step % 2 == 0:
+                lower.append(lax.ppermute(lower[-1] if lower else normed, "tp", pairs_2))
+            else:
+                upper.append(lax.ppermute(upper[-1] if upper else normed, "tp", back))
+        blocks = jnp.stack([*lower[::-1], normed, *upper])
+        shift = lax.axis_index("tp") - len(lower)
+        blocks = blocks[(jnp.arange(devices) - shift) % devices]
+        tokens = joined_along(blocks, 0)
         empty = jnp.zeros((tokens.shape[0], chans), jnp.float32)
 
         def add_both(totals, pieces, start, tokens=tokens):

time: 363 us -> 309 us (0.85)
  waiting for transfers between devices: 177 us -> 101 us
  starting transfers between devices: 10.8 us -> 57.5 us
  blocking collectives: 124 us -> 78.7 us
  local copies, waits for them, and re-layouts: 7.75 us -> 26.1 us
    all_gather x2 -> x0, waiting for transfers between devices: 68.5 us -> none  [body(): tokens = lax.all_gather(normed, 'tp', axis=0, tiled=True)]
    all_to_all x2 -> x1, blocking collectives: 93.5 us -> 47.2 us  [sum_at_owner(): lax.all_to_all(tiles, axis, split_axis=0, concat_axis=0, tiled=True)]
    all_gather x2, waiting for transfers between devices: 75.5 us -> 29.7 us  [sent_together(): whole = lax.all_gather(both, axis, axis=dim, tiled=True)]
    all_to_all x0 -> x1, waiting for transfers between devices: none -> 36 us  [sum_at_owner(): lax.all_to_all(tiles, axis, split_axis=0, concat_axis=0, tiled=True)]
    ppermute x0 -> x14, starting transfers between devices: none -> 32.3 us  [the longest x8 18.8 us: body(): lower.append(lax.ppermute(lower[-1] if lower else normed, 'tp', pairs_2))]
    ppermute x0 -> x14, waiting for transfers between devices: none -> 18.1 us  [the longest x8 14.6 us: body(): lower.append(lax.ppermute(lower[-1] if lower else normed, 'tp', pairs_2))]
    all_gather x2, waiting for transfers between devices: 27.6 us -> 12.1 us  [whole_of(): nearer = lax.all_gather(shard, axes[-1], axis=dim, tiled=True)]
    all_to_all x0 -> x1, starting transfers between devices: none -> 9.95 us  [sum_at_owner(): lax.all_to_all(tiles, axis, split_axis=0, concat_axis=0, tiled=True)]
  transfers between devices with their start and end apart: 9 -> 22, of which waited for: 8 -> 14; matrix products, arithmetic and copies ran while one was open for 8% -> 14% of each run, Pallas kernels for 0% -> 0%
where the time goes in v1:
time: 309 us; the launch traced here: 307 us
  waiting for transfers between devices  101 us (33%)
  blocking collectives  78.7 us (25%)
  starting transfers between devices  57.5 us (19%)
  local copies, waits for them, and re-layouts  26.1 us (8%)
  other arithmetic  14.9 us (5%)
  matrix products  14.9 us (5%)
  between operations  14.3 us (5%)
    all_to_all x1, blocking collectives, sum_at_owner(): lax.all_to_all(tiles, axis, split_axis=0, concat_axis=0, tiled=True)  47.2 us
    all_to_all x1, waiting for transfers between devices, sum_at_owner(): lax.all_to_all(tiles, axis, split_axis=0, concat_axis=0, tiled=True)  36 us
    all_gather x2, waiting for transfers between devices, sent_together(): whole = lax.all_gather(both, axis, axis=dim, tiled=True)  29.7 us
    all_gather x2, blocking collectives, whole_of(): nearer = lax.all_gather(shard, axes[-1], axis=dim, tiled=True)  21.6 us
    ppermute x8, starting transfers between devices, body(): lower.append(lax.ppermute(lower[-1] if lower else normed, 'tp', pairs_2))  18.8 us
    ppermute x8, waiting for transfers between devices, body(): lower.append(lax.ppermute(lower[-1] if lower else normed, 'tp', pairs_2))  14.6 us
    ppermute x6, starting transfers between devices, body(): upper.append(lax.ppermute(upper[-1] if upper else normed, 'tp', back))  13.5 us
    all_gather x2, waiting for transfers between devices, whole_of(): nearer = lax.all_gather(shard, axes[-1], axis=dim, tiled=True)  12.1 us
  transfers between devices with their start and end apart: 22, of which 14 were waited for; matrix products, arithmetic and copies ran while one was open for 14% of the time, Pallas kernels for 0%

profile of v1, /device:TPU:1, one launch (start us, length us, event | category | flops | bytes accessed | tf_op | source)
XLA Modules:
  0.0 307.4 jit_solution(10079257578309725555)
XLA Ops:
  11.9 2.6 collective-permute-start
  15.1 4.1 %collective-permute-done = bf16[96,2048]{1,0:T(8,128)(2,1)S(1)} collective-permute-done((bf16[96,2048]{1,0:T(8,128)(2,1)S(1)}, bf16[96,2048]{1,0:T(8,128)(2,1)S(1)}, u32[]{:S(2)}, u32[]{:S(2)}) %collective-permute-start) | collective-permute-done | bytes 393248 | tf_op jit(solution)/shard_map/ppermute | solution.py:87
  19.2 2.5 collective-permute-start.1
  23.1 10.7 %all-gather = bf16[1,256,256]{1,2,0:T(8,128)(2,1)} all-gather(bf16[1,256,64]{1,2,0:T(8,128)(2,1)S(1)} %get-tuple-element.17), channel_id=2, replica_groups=mesh['sp_0'=8,'sp_1'=4,'tp'=8] {'sp_1'}, dimensions={2}, use_global_device_ids=true | all-gather | bytes 163840 | tf_op jit(solution)/shard_map/all_gather | solution.py:55
  34.5 2.6 collective-permute-start.2
  41.8 2.5 collective-permute-start.3
  52.1 2.7 collective-permute-done.6
  54.9 2.5 gather_fusion
  57.4 29.7 %all-gather.9.cloned.1.call-done = bf16[2048,512]{1,0:T(8,128)(2,1)} async-done(((bf16[64,512]{1,0:T(8,128)(2,1)}), bf16[2048,512]{1,0:T(8,128)(2,1)}) %all-gather.9.cloned.1.call-update) | async-done | bytes 2097168 | tf_op jit(solution)/shard_map/all_gather | solution.py:21
  87.1 3.3 %fusion.3 = f32[768,256]{1,0:T(8,128)S(1)} fusion(bf16[768,2048]{1,0:T(8,128)(2,1)} %bitcast.129, bf16[2048,512]{1,0:T(8,128)(2,1)} %all-gather.9.cloned.1.call-done), kind=kOutput, calls=%fused_computation.13 | convolution fusion | flops 805896192 | bytes 4980736 | tf_op jit(solution)/shard_map/dot_general | solution.py:99
  95.8 3.5 %fusion.105 = (f32[768]{0:T(1024)S(1)}, f32[768]{0:T(1024)S(1)}, f32[768,256]{1,0:T(8,128)S(1)}) fusion(f32[798,256]{1,0:T(8,128)S(1)} %maximum_convert_fusion, f32[256]{0:T(256)S(1)} %bitcast.170, f32[256]{0:T(256)S(1)} %bitcast.171, f32[256]{0:T(256)S(1)} %bitcast.172, f32[256]{0:T(256)S(1)} %bitcast.173, f32[256]{0:T(256)S(1)} %bitcast.174, ...), kind=kLoop, calls=%fused_computation.224 | loop fusion | flops 12777984 | bytes 25204736 | tf_op jit(solution)/shard_map/reduce_sum | solution.py:112
  100.0 9.9 %all-to-all-start = ((f32[8,1,1536]{2,1,0:T(1,128)}), f32[8,1,1536]{2,1,0:T(1,128)S(1)}, u32[]{:S(2)}, u32[]{:S(2)}) async-start(f32[8,1,1536]{2,1,0:T(1,128)} %broadcast_in_dim.4), calls=%async_computation | async-start | bytes 98304 | tf_op jit(solution)/shard_map/all_to_all | solution.py:33
  110.5 4.2 %all-to-all-done = f32[8,1,1536]{2,1,0:T(1,128)S(1)} async-done(((f32[8,1,1536]{2,1,0:T(1,128)}), f32[8,1,1536]{2,1,0:T(1,128)S(1)}, u32[]{:S(2)}, u32[]{:S(2)}) %all-to-all-start) | async-done | bytes 49184 | tf_op jit(solution)/shard_map/all_to_all | solution.py:33
  114.8 9.3 %all-gather.13.cloned.1.call-done = bf16[1,256,2048]{1,2,0:T(8,128)(2,1)} async-done(((bf16[1,256,256]{1,2,0:T(8,128)(2,1)}), bf16[1,256,2048]{1,2,0:T(8,128)(2,1)}) %all-gather.13.cloned.1.call-update) | async-done | bytes 1048592 | tf_op jit(solution)/shard_map/all_gather | solution.py:55
  124.1 4.0 %convolution_convert_fusion.1 = bf16[768,2048]{1,0:T(8,128)(2,1)} fusion(bf16[1,256,2048]{1,2,0:T(8,128)(2,1)} %all-gather.13.cloned.1.call-done, f32[768,256]{1,0:T(8,128)S(1)} %get-tuple-element.12, f32[256]{0:T(256)S(1)} %bitcast.203, f32[256]{0:T(256)S(1)} %bitcast.202, f32[768]{0:T(1024)S(1)} %get-tuple-element.86, f32[768]{0:T(1024)S(1)} %get-tuple-element.85), kind=kOutput, calls=%fused_computation.5 | convolution fusion | flops 808648704 | bytes 4988928 | tf_op jit(solution)/shard_map/dot_general | solution.py:122
  128.1 10.0 %all-to-all-start.1 = ((bf16[8,96,2048]{2,1,0:T(8,128)(2,1)}), bf16[8,96,2048]{2,1,0:T(8,128)(2,1)S(1)}, u32[]{:S(2)}, u32[]{:S(2)}) async-start(bf16[8,96,2048]{2,1,0:T(8,128)(2,1)} %bitcast.126), calls=%async_computation.1 | async-start | bytes 6291456 | tf_op jit(solution)/shard_map/all_to_all | solution.py:67
  139.5 36.0 %all-to-all-done.1 = bf16[8,96,2048]{2,1,0:T(8,128)(2,1)S(1)} async-done(((bf16[8,96,2048]{2,1,0:T(8,128)(2,1)}), bf16[8,96,2048]{2,1,0:T(8,128)(2,1)S(1)}, u32[]{:S(2)}, u32[]{:S(2)}) %all-to-all-start.1) | async-done | bytes 3145760 | tf_op jit(solution)/shard_map/all_to_all | solution.py:67
  177.6 4.7 %collective-permute-done.8 = bf16[96,2048]{1,0:T(8,128)(2,1)S(1)} collective-permute-done((bf16[96,2048]{1,0:T(8,128)(2,1)S(1)}, bf16[96,2048]{1,0:T(8,128)(2,1)S(1)}, u32[]{:S(2)}, u32[]{:S(2)}) %collective-permute-start.8) | collective-permute-done | bytes 393248 | tf_op jit(solution)/shard_map/ppermute | solution.py:87
  183.1 2.5 collective-permute-start.9
  186.6 3.7 %collective-permute-done.9 = bf16[96,2048]{1,0:T(8,128)(2,1)S(1)} collective-permute-done((bf16[96,2048]{1,0:T(8,128)(2,1)S(1)}, bf16[96,2048]{1,0:T(8,128)(2,1)S(1)}, u32[]{:S(2)}, u32[]{:S(2)}) %collective-permute-start.9) | collective-permute-done | bytes 393248 | tf_op jit(solution)/shard_map/ppermute | solution.py:87
  190.3 2.5 collective-permute-start.10
  193.2 2.6 collective-permute-start.13
  197.5 2.5 collective-permute-start.11
  200.0 10.9 %all-gather.2 = bf16[1,256,256]{1,2,0:T(8,128)(2,1)} all-gather(bf16[1,256,64]{1,2,0:T(8,128)(2,1)S(1)} %copy-done.12), channel_id=4, replica_groups=mesh['sp_0'=8,'sp_1'=4,'tp'=8] {'sp_1'}, dimensions={2}, use_global_device_ids=true | all-gather | bytes 163840 | tf_op jit(solution)/shard_map/all_gather | solution.py:55
  210.9 5.7 %collective-permute-start.14 = (bf16[96,2048]{1,0:T(8,128)(2,1)}, bf16[96,2048]{1,0:T(8,128)(2,1)S(1)}, u32[]{:S(2)}, u32[]{:S(2)}) collective-permute-start(bf16[96,2048]{1,0:T(8,128)(2,1)} %collective-permute-done.13), channel_id=1, source_target_pairs={{1,0},{2,1},{3,2},{4,3},{5,4},{6,5},{7,6},{0,7},{9,8},{10,9},{11,1... | collective-permute-start | bytes 1179656 | tf_op jit(solution)/shard_map/ppermute | solution.py:89
  222.1 2.5 gather_fusion.1
  224.6 3.3 %fusion.5 = f32[768,256]{1,0:T(8,128)S(1)} fusion(bf16[768,2048]{1,0:T(8,128)(2,1)} %bitcast.127, bf16[2048,512]{1,0:T(8,128)(2,1)} %all-gather.11.cloned.1.call-done), kind=kOutput, calls=%fused_computation.15 | convolution fusion | flops 805896192 | bytes 4980736 | tf_op jit(solution)/shard_map/dot_general | solution.py:99
  229.6 2.9 collective-permute-start.15
  233.7 3.5 %fusion.104 = (f32[768]{0:T(1024)S(1)}, f32[768]{0:T(1024)S(1)}, f32[768,256]{1,0:T(8,128)S(1)}) fusion(f32[798,256]{1,0:T(8,128)S(1)} %maximum_convert_fusion.1, f32[256]{0:T(256)S(1)} %bitcast.136, f32[256]{0:T(256)S(1)} %bitcast.137, f32[256]{0:T(256)S(1)} %bitcast.180, f32[256]{0:T(256)S(1)} %bitcast.181, f32[256]{0:T(256)S(1)} %bitcast.182, ...), kind=kLoop, calls=%fused_computation.223 | loop fusion | flops 12777984 | bytes 25204736 | tf_op jit(solution)/shard_map/reduce_sum | solution.py:112
  237.2 9.9 %all_to_all.22 = f32[8,1,1536]{2,1,0:T(1,128)S(1)} all-to-all(f32[8,1,1536]{2,1,0:T(1,128)S(1)} %broadcast_in_dim.5), channel_id=1, replica_groups=mesh['sp_0'=8,'sp_1'=4,'tp'=8] {'tp'}, dimensions={0} | all-to-all | bytes 98304 | tf_op jit(solution)/shard_map/all_to_all | solution.py:33
  247.2 2.8 all-gather.15.cloned.1.call-done
  252.3 47.2 %all_to_all.23 = bf16[8,96,2048]{2,1,0:T(8,128)(2,1)S(1)} all-to-all(bf16[8,96,2048]{2,1,0:T(8,128)(2,1)S(1)} %bitcast.131), channel_id=1, replica_groups=mesh['sp_0'=8,'sp_1'=4,'tp'=8] {'tp'}, dimensions={0} | all-to-all | bytes 6291456 | tf_op jit(solution)/shard_map/all_to_all | solution.py:67
  (211 shorter events, 45.9 us)
Async XLA Ops:
  6.5 45.3 %copy-start = (bf16[96,2048]{1,0:T(8,128)(2,1)S(1)}, bf16[96,2048]{1,0:T(8,128)(2,1)}, u32[]{:S(2)}) copy-start(bf16[96,2048]{1,0:T(8,128)(2,1)} %param.9) | copy-start | bytes 1179652
  6.5 80.5 %all-gather.9.cloned.1.call-start = ((), (), s32[]{:S(2)}) async-start(), calls=%async_computation.4 | async-start | bytes 2162688 | tf_op jit(solution)/shard_map/all_gather | solution.py:21
  8.7 115.4 %all-gather.13.cloned.1.call-start = ((), (), s32[]{:S(2)}) async-start(), calls=%async_computation.6 | async-start | bytes 1179648 | tf_op jit(solution)/shard_map/all_gather | solution.py:55
  11.9 7.3 %collective-permute-start = (bf16[96,2048]{1,0:T(8,128)(2,1)S(1)}, bf16[96,2048]{1,0:T(8,128)(2,1)S(1)}, u32[]{:S(2)}, u32[]{:S(2)}) collective-permute-start(bf16[96,2048]{1,0:T(8,128)(2,1)S(1)} %fusion.16), channel_id=1, source_target_pairs={{0,1},{1,2},{2,3},{3,4},{4,5},{5,6},{6,7},{7,0},{8,9},{9,10},{10,1... | collective-permute-start | bytes 1179656 | tf_op jit(solution)/shard_map/ppermute | solution.py:87
  14.5 25.5 %collective-permute-start.4 = (bf16[96,2048]{1,0:T(8,128)(2,1)S(1)}, bf16[96,2048]{1,0:T(8,128)(2,1)S(1)}, u32[]{:S(2)}, u32[]{:S(2)}) collective-permute-start(bf16[96,2048]{1,0:T(8,128)(2,1)S(1)} %fusion.16), channel_id=1, source_target_pairs={{1,0},{2,1},{3,2},{4,3},{5,4},{6,5},{7,6},{0,7},{9,8},{10,9},{11,1... | collective-permute-start | bytes 1179656 | tf_op jit(solution)/shard_map/ppermute | solution.py:89
  19.2 30.5 %copy-start.5 = (bf16[96,2048]{1,0:T(8,128)(2,1)}, bf16[96,2048]{1,0:T(8,128)(2,1)S(1)}, u32[]{:S(2)}) copy-start(bf16[96,2048]{1,0:T(8,128)(2,1)S(1)} %collective-permute-done) | copy-start | bytes 1179652
  19.2 15.2 %collective-permute-start.1 = (bf16[96,2048]{1,0:T(8,128)(2,1)S(1)}, bf16[96,2048]{1,0:T(8,128)(2,1)S(1)}, u32[]{:S(2)}, u32[]{:S(2)}) collective-permute-start(bf16[96,2048]{1,0:T(8,128)(2,1)S(1)} %collective-permute-done), channel_id=1, source_target_pairs={{0,1},{1,2},{2,3},{3,4},{4,5},{5,6},{6,7},{7,0},{8,9},{9,10},{10,1... | collective-permute-start | bytes 1179656 | tf_op jit(solution)/shard_map/ppermute | solution.py:87
  33.8 18.0 %copy-start.61 = (f32[96]{0:T(128)S(1)}, f32[96]{0:T(128)}, u32[]{:S(2)}) copy-start(f32[96]{0:T(128)} %copy-done.60) | copy-start | bytes 1156
  34.5 15.2 %copy-start.6 = (bf16[96,2048]{1,0:T(8,128)(2,1)}, bf16[96,2048]{1,0:T(8,128)(2,1)S(1)}, u32[]{:S(2)}) copy-start(bf16[96,2048]{1,0:T(8,128)(2,1)S(1)} %collective-permute-done.1) | copy-start | bytes 1179652
  34.5 7.4 %collective-permute-start.2 = (bf16[96,2048]{1,0:T(8,128)(2,1)S(1)}, bf16[96,2048]{1,0:T(8,128)(2,1)S(1)}, u32[]{:S(2)}, u32[]{:S(2)}) collective-permute-start(bf16[96,2048]{1,0:T(8,128)(2,1)S(1)} %collective-permute-done.1), channel_id=1, source_target_pairs={{0,1},{1,2},{2,3},{3,4},{4,5},{5,6},{6,7},{7,0},{8,9},{9,10},{10,1... | collective-permute-start | bytes 1179656 | tf_op jit(solution)/shard_map/ppermute | solution.py:87
  40.0 9.7 %copy-start.3 = (bf16[96,2048]{1,0:T(8,128)(2,1)}, bf16[96,2048]{1,0:T(8,128)(2,1)S(1)}, u32[]{:S(2)}) copy-start(bf16[96,2048]{1,0:T(8,128)(2,1)S(1)} %collective-permute-done.4) | copy-start | bytes 1179652
  40.0 7.6 %collective-permute-start.5 = (bf16[96,2048]{1,0:T(8,128)(2,1)S(1)}, bf16[96,2048]{1,0:T(8,128)(2,1)S(1)}, u32[]{:S(2)}, u32[]{:S(2)}) collective-permute-start(bf16[96,2048]{1,0:T(8,128)(2,1)S(1)} %collective-permute-done.4), channel_id=1, source_target_pairs={{1,0},{2,1},{3,2},{4,3},{5,4},{6,5},{7,6},{0,7},{9,8},{10,9},{11,1... | collective-permute-start | bytes 1179656 | tf_op jit(solution)/shard_map/ppermute | solution.py:89
  41.8 7.9 %collective-permute-start.3 = (bf16[96,2048]{1,0:T(8,128)(2,1)S(1)}, bf16[96,2048]{1,0:T(8,128)(2,1)S(1)}, u32[]{:S(2)}, u32[]{:S(2)}) collective-permute-start(bf16[96,2048]{1,0:T(8,128)(2,1)S(1)} %collective-permute-done.2), channel_id=1, source_target_pairs={{0,1},{1,2},{2,3},{3,4},{4,5},{5,6},{6,7},{7,0},{8,9},{9,10},{10,1... | collective-permute-start | bytes 1179656 | tf_op jit(solution)/shard_map/ppermute | solution.py:87
  47.6 7.2 %collective-permute-start.6 = (bf16[96,2048]{1,0:T(8,128)(2,1)S(1)}, bf16[96,2048]{1,0:T(8,128)(2,1)S(1)}, u32[]{:S(2)}, u32[]{:S(2)}) collective-permute-start(bf16[96,2048]{1,0:T(8,128)(2,1)S(1)} %collective-permute-done.5), channel_id=1, source_target_pairs={{1,0},{2,1},{3,2},{4,3},{5,4},{6,5},{7,6},{0,7},{9,8},{10,9},{11,1... | collective-permute-start | bytes 1179656 | tf_op jit(solution)/shard_map/ppermute | solution.py:89
  92.2 3.2 %collective-permute-start.7 = (bf16[30,256]{1,0:T(8,128)(2,1)S(1)}, bf16[30,256]{1,0:T(8,128)(2,1)S(1)}, u32[]{:S(2)}, u32[]{:S(2)}) collective-permute-start(bf16[30,256]{1,0:T(8,128)(2,1)S(1)} %slice.580), channel_id=1, source_target_pairs={{0,8},{8,16},{16,24},{24,32},{32,40},{40,48},{48,56},{56,64},{64,7... | collective-permute-start | bytes 46088 | tf_op jit(solution)/shard_map/ppermute | solution.py:28
  95.8 14.1 %copy-start.59 = (f32[2,256]{1,0:T(2,128)S(1)}, f32[2,256]{1,0:T(2,128)}, u32[]{:S(2)}) copy-start(f32[2,256]{1,0:T(2,128)} %param.16) | copy-start | bytes 6148
  100.0 14.7 %all-to-all-start = ((f32[8,1,1536]{2,1,0:T(1,128)}), f32[8,1,1536]{2,1,0:T(1,128)S(1)}, u32[]{:S(2)}, u32[]{:S(2)}) async-start(f32[8,1,1536]{2,1,0:T(1,128)} %broadcast_in_dim.4), calls=%async_computation | async-start | bytes 98304 | tf_op jit(solution)/shard_map/all_to_all | solution.py:33
  128.1 47.4 %all-to-all-start.1 = ((bf16[8,96,2048]{2,1,0:T(8,128)(2,1)}), bf16[8,96,2048]{2,1,0:T(8,128)(2,1)S(1)}, u32[]{:S(2)}, u32[]{:S(2)}) async-start(bf16[8,96,2048]{2,1,0:T(8,128)(2,1)} %bitcast.126), calls=%async_computation.1 | async-start | bytes 6291456 | tf_op jit(solution)/shard_map/all_to_all | solution.py:67
  138.1 86.6 %all-gather.11.cloned.1.call-start = ((), (), s32[]{:S(2)}) async-start(), calls=%async_computation.5 | async-start | bytes 2162688 | tf_op jit(solution)/shard_map/all_gather | solution.py:21
  139.5 110.5 %all-gather.15.cloned.1.call-start = ((), (), s32[]{:S(2)}) async-start(), calls=%async_computation.7 | async-start | bytes 1179648 | tf_op jit(solution)/shard_map/all_gather | solution.py:55
  175.5 24.5 %copy-start.12 = (bf16[1,256,64]{1,2,0:T(8,128)(2,1)S(1)}, bf16[1,256,64]{1,2,0:T(8,128)(2,1)}, u32[]{:S(2)}) copy-start(bf16[1,256,64]{1,2,0:T(8,128)(2,1)} %get-tuple-element.18) | copy-start | bytes 98308
  176.5 5.9 %collective-permute-start.8 = (bf16[96,2048]{1,0:T(8,128)(2,1)S(1)}, bf16[96,2048]{1,0:T(8,128)(2,1)S(1)}, u32[]{:S(2)}, u32[]{:S(2)}) collective-permute-start(bf16[96,2048]{1,0:T(8,128)(2,1)S(1)} %fusion.20), channel_id=1, source_target_pairs={{0,1},{1,2},{2,3},{3,4},{4,5},{5,6},{6,7},{7,0},{8,9},{9,10},{10,1... | collective-permute-start | bytes 1179656 | tf_op jit(solution)/shard_map/ppermute | solution.py:87
  183.1 7.2 %collective-permute-start.9 = (bf16[96,2048]{1,0:T(8,128)(2,1)S(1)}, bf16[96,2048]{1,0:T(8,128)(2,1)S(1)}, u32[]{:S(2)}, u32[]{:S(2)}) collective-permute-start(bf16[96,2048]{1,0:T(8,128)(2,1)S(1)} %collective-permute-done.8), channel_id=1, source_target_pairs={{0,1},{1,2},{2,3},{3,4},{4,5},{5,6},{6,7},{7,0},{8,9},{9,10},{10,1... | collective-permute-start | bytes 1179656 | tf_op jit(solution)/shard_map/ppermute | solution.py:87
  185.6 7.6 %collective-permute-start.12 = (bf16[96,2048]{1,0:T(8,128)(2,1)S(1)}, bf16[96,2048]{1,0:T(8,128)(2,1)S(1)}, u32[]{:S(2)}, u32[]{:S(2)}) collective-permute-start(bf16[96,2048]{1,0:T(8,128)(2,1)S(1)} %fusion.20), channel_id=1, source_target_pairs={{1,0},{2,1},{3,2},{4,3},{5,4},{6,5},{7,6},{0,7},{9,8},{10,9},{11,1... | collective-permute-start | bytes 1179656 | tf_op jit(solution)/shard_map/ppermute | solution.py:89
  190.3 7.2 %collective-permute-start.10 = (bf16[96,2048]{1,0:T(8,128)(2,1)S(1)}, bf16[96,2048]{1,0:T(8,128)(2,1)S(1)}, u32[]{:S(2)}, u32[]{:S(2)}) collective-permute-start(bf16[96,2048]{1,0:T(8,128)(2,1)S(1)} %collective-permute-done.9), channel_id=1, source_target_pairs={{0,1},{1,2},{2,3},{3,4},{4,5},{5,6},{6,7},{7,0},{8,9},{9,10},{10,1... | collective-permute-start | bytes 1179656 | tf_op jit(solution)/shard_map/ppermute | solution.py:87
  193.2 23.5 %copy-start.8 = (bf16[96,2048]{1,0:T(8,128)(2,1)}, bf16[96,2048]{1,0:T(8,128)(2,1)S(1)}, u32[]{:S(2)}) copy-start(bf16[96,2048]{1,0:T(8,128)(2,1)S(1)} %collective-permute-done.12) | copy-start | bytes 1179652
  193.2 17.7 %collective-permute-start.13 = (bf16[96,2048]{1,0:T(8,128)(2,1)S(1)}, bf16[96,2048]{1,0:T(8,128)(2,1)}, u32[]{:S(2)}, u32[]{:S(2)}) collective-permute-start(bf16[96,2048]{1,0:T(8,128)(2,1)S(1)} %collective-permute-done.12), channel_id=1, source_target_pairs={{1,0},{2,1},{3,2},{4,3},{5,4},{6,5},{7,6},{0,7},{9,8},{10,9},{11,1... | collective-permute-start | bytes 1179656 | tf_op jit(solution)/shard_map/ppermute | solution.py:89
  197.5 19.2 %copy-start.11 = (bf16[96,2048]{1,0:T(8,128)(2,1)}, bf16[96,2048]{1,0:T(8,128)(2,1)S(1)}, u32[]{:S(2)}) copy-start(bf16[96,2048]{1,0:T(8,128)(2,1)S(1)} %collective-permute-done.10) | copy-start | bytes 1179652
  197.5 19.2 %collective-permute-start.11 = (bf16[96,2048]{1,0:T(8,128)(2,1)S(1)}, bf16[96,2048]{1,0:T(8,128)(2,1)}, u32[]{:S(2)}, u32[]{:S(2)}) collective-permute-start(bf16[96,2048]{1,0:T(8,128)(2,1)S(1)} %collective-permute-done.10), channel_id=1, source_target_pairs={{0,1},{1,2},{2,3},{3,4},{4,5},{5,6},{6,7},{7,0},{8,9},{9,10},{10,1... | collective-permute-start | bytes 1179656 | tf_op jit(solution)/shard_map/ppermute | solution.py:87
  210.9 11.1 %collective-permute-start.14 = (bf16[96,2048]{1,0:T(8,128)(2,1)}, bf16[96,2048]{1,0:T(8,128)(2,1)S(1)}, u32[]{:S(2)}, u32[]{:S(2)}) collective-permute-start(bf16[96,2048]{1,0:T(8,128)(2,1)} %collective-permute-done.13), channel_id=1, source_target_pairs={{1,0},{2,1},{3,2},{4,3},{5,4},{6,5},{7,6},{0,7},{9,8},{10,9},{11,1... | collective-permute-start | bytes 1179656 | tf_op jit(solution)/shard_map/ppermute | solution.py:89
  229.6 3.8 %collective-permute-start.15 = (bf16[30,256]{1,0:T(8,128)(2,1)S(1)}, bf16[30,256]{1,0:T(8,128)(2,1)S(1)}, u32[]{:S(2)}, u32[]{:S(2)}) collective-permute-start(bf16[30,256]{1,0:T(8,128)(2,1)S(1)} %slice.614), channel_id=1, source_target_pairs={{0,8},{8,16},{16,24},{24,32},{32,40},{40,48},{48,56},{56,64},{64,7... | collective-permute-start | bytes 46088 | tf_op jit(solution)/shard_map/ppermute | solution.py:28
  233.7 16.3 %copy-start.62 = (f32[1,256]{1,0:T(1,128)S(1)}, f32[1,256]{1,0:T(1,128)}, u32[]{:S(2)}) copy-start(f32[1,256]{1,0:T(1,128)} %get-tuple-element.89) | copy-start | bytes 3076
  (55 other events, 252.0 us)
Sparse Core Ops, SparseCore 0:
  9.9 77.1 all-gather.8
  88.9 35.2 all-gather.12
  141.4 71.6 all-gather.10
  214.7 35.1 all-gather.14
